TPU v7x, 32 devices: a whole 2x2x4 slice. The times are simulated.
32 devices in a mesh: sp: 4 (over x, core), dp: 8 (over z, y).
Axes of the slice: x: 2, y: 2, z: 4, core: 2. Of those that a mesh axis runs over, the one named last changes fastest.
Arguments:
- queries: bfloat16 [16, 8, 576, 128], P('dp', None, 'sp'), may hold values from -6 to 6
- keys: bfloat16 [16, 8, 576, 128], P('dp', None, 'sp'), may hold values from -6 to 6
- values: bfloat16 [16, 8, 576, 128], P('dp', None, 'sp'), may hold values from -6 to 6
- in_gate: bfloat16 [16, 8, 576], P('dp', None, 'sp'), may hold values from -5 to 240
- forget_gate: bfloat16 [16, 8, 576], P('dp', None, 'sp'), may hold values from 1 to 20
- out_gate: bfloat16 [16, 8, 576, 128], P('dp', None, 'sp'), may hold values from -6 to 6
- norm_gain: float32 [8, 128], replicated, may hold values from 0.1 to 1.9
- out_weight: bfloat16 [1024, 2048], P(None, 'dp'), may hold values from -0.1875 to 0.1875
Outputs:
- mixed: bfloat16 [16, 576, 2048], P('dp', 'sp')
All inputs are finite; a program needn't handle non-finite values.
Results may differ from a plain program's by a relative error of at most 0.0057.
Values may be sent and summed in bfloat16 or wider, within the bound.
A program may use at most 64 MiB of HBM per device.

v0:
```python
import jax
import jax.numpy as jnp
from jax import lax
from jax.sharding import PartitionSpec as P

BLK = 64


highest = lax.Precision.HIGHEST
norm_eps = 1e-05


def run_cells(parts):
    query_in, key_in, value_in, input_in, forget_in = parts
    item_count = query_in.shape[1]
    seq_len = query_in.shape[2]
    head_size = query_in.shape[3]
    blocks = seq_len // BLK
    key_scale = head_size ** (-0.5)
    query_b = query_in.reshape(item_count, blocks, BLK, head_size)
    key_b = key_in.reshape(item_count, blocks, BLK, head_size)
    value_b = value_in.reshape(item_count, blocks, BLK, head_size)
    input_b = input_in.astype(jnp.float32).reshape(item_count, blocks, BLK)
    logf_b = jax.nn.log_sigmoid(forget_in.astype(jnp.float32)).reshape(item_count, blocks, BLK)
    cumulative = jnp.cumsum(logf_b, axis=-1)
    block_end = cumulative[..., -1]
    growth = block_end[..., None] - cumulative + input_b
    growth_max = jnp.max(growth, axis=-1)
    w_key = jnp.exp(growth - growth_max[..., None]) * key_scale
    key_f = key_b.astype(jnp.float32)
    value_f = value_b.astype(jnp.float32)
    weighted = w_key[..., None] * key_f
    fresh_memory = jnp.einsum("ncsd,ncse->ncde", weighted, value_f, precision=highest)
    fresh_norm = jnp.sum(weighted, axis=2)

    def advance(state_in, inputs):
        memory, normalizer, stabilizer = state_in
        end_now, top_now, memory_add, norm_add = inputs
        stab_new = jnp.maximum(end_now + stabilizer, top_now)
        decay_old = jnp.exp(end_now + stabilizer - stab_new)
        decay_add = jnp.exp(top_now - stab_new)
        memory_new = decay_old[:, None, None] * memory + decay_add[:, None, None] * memory_add
        norm_new = decay_old[:, None] * normalizer + decay_add[:, None] * norm_add
        return ((memory_new, norm_new, stab_new), (memory, normalizer, stabilizer))

    start = (
        jnp.zeros((item_count, head_size, head_size), jnp.float32),
        jnp.zeros((item_count, head_size), jnp.float32),
        jnp.zeros((item_count,), jnp.float32),
    )
    series = (
        jnp.swapaxes(block_end, 0, 1),
        jnp.swapaxes(growth_max, 0, 1),
        jnp.swapaxes(fresh_memory, 0, 1),
        jnp.swapaxes(fresh_norm, 0, 1),
    )
    _, (memory_prev, norm_prev, stab_prev) = lax.scan(advance, start, series)
    memory_prev = jnp.swapaxes(memory_prev, 0, 1)
    norm_prev = jnp.swapaxes(norm_prev, 0, 1)
    stab_prev = jnp.swapaxes(stab_prev, 0, 1)
    causal_mask = jnp.tril(jnp.ones((BLK, BLK), dtype=bool))
    log_weights = cumulative[..., :, None] - cumulative[..., None, :] + input_b[..., None, :]
    log_weights = jnp.where(causal_mask, log_weights, -jnp.inf)
    carried_log = cumulative + stab_prev[..., None]
    row_max = jnp.maximum(jnp.max(log_weights, axis=-1), carried_log)
    w_intra = jnp.exp(log_weights - row_max[..., None])
    w_inter = jnp.exp(carried_log - row_max)
    scores = jnp.einsum("ncpd,ncqd->ncpq", query_b, key_b, preferred_element_type=jnp.float32) * (
        key_scale * w_intra
    )
    query_f = query_b.astype(jnp.float32)
    numerator = w_inter[..., None] * jnp.einsum(
        "ncpd,ncde->ncpe", query_f, memory_prev, precision=highest
    )
    numerator = numerator + jnp.einsum("ncpq,ncqe->ncpe", scores, value_f, precision=highest)
    denominator = w_inter * jnp.einsum(
        "ncpd,ncd->ncp", query_f, norm_prev, precision=highest
    ) + jnp.sum(scores, axis=-1)
    cell_out = numerator / jnp.maximum(jnp.abs(denominator), 1.0)[..., None]
    return cell_out.reshape(1, item_count, seq_len, head_size).astype(jnp.bfloat16)


def body(queries, keys, values, in_gate, forget_gate, out_gate, norm_gain, out_weight):
    rank_count = lax.axis_size("sp")
    group_seqs, head_count, span_len, head_size = queries.shape

    def by_rank(array):
        return array.reshape((rank_count, -1) + array.shape[2:])

    cell_out = run_cells(
        (
            lax.all_to_all(by_rank(queries), "sp", split_axis=0, concat_axis=2, tiled=True),
            lax.all_to_all(by_rank(keys), "sp", split_axis=0, concat_axis=2, tiled=True),
            lax.all_to_all(by_rank(values), "sp", split_axis=0, concat_axis=2, tiled=True),
            lax.all_to_all(by_rank(in_gate), "sp", split_axis=0, concat_axis=2, tiled=True),
            lax.all_to_all(by_rank(forget_gate), "sp", split_axis=0, concat_axis=2, tiled=True),
        )
    )
    returned = lax.all_to_all(cell_out, "sp", split_axis=2, concat_axis=0, tiled=True)
    returned = returned.reshape(group_seqs, head_count, span_len, head_size).astype(jnp.float32)
    mean_val = jnp.mean(returned, axis=-1, keepdims=True)
    centered = returned - mean_val
    variance = jnp.mean(centered * centered, axis=-1, keepdims=True)
    normed = centered * lax.rsqrt(variance + norm_eps) * norm_gain[None, :, None, :]
    hidden = (normed * jax.nn.sigmoid(out_gate.astype(jnp.float32))).astype(jnp.bfloat16)
    hidden = jnp.swapaxes(hidden, 1, 2).reshape(group_seqs * span_len, head_count * head_size)
    result = jnp.dot(
        hidden,
        lax.all_gather(out_weight, "dp", axis=1, tiled=True),
        preferred_element_type=jnp.float32,
    )
    return result.astype(jnp.bfloat16).reshape(group_seqs, span_len, -1)


def solution(mesh):
    return jax.shard_map(
        body,
        mesh=mesh,
        in_specs=(
            P("dp", None, "sp", None),
            P("dp", None, "sp", None),
            P("dp", None, "sp", None),
            P("dp", None, "sp"),
            P("dp", None, "sp"),
            P("dp", None, "sp", None),
            P(),
            P(None, "dp"),
        ),
        out_specs=P("dp", "sp", None),
        check_vma=False,
    )
```

profile of v0, /device:TPU:0, one launch (start us, length us, event | category | flops | bytes accessed | tf_op | source)
XLA Modules:
  0.0 103.2 jit_solution(3290982956562113304)
XLA Ops:
  6.5 1.3 %reshape.170 = bf16[4,4,144]{2,1,0:T(4,128)(2,1)} reshape(bf16[2,8,144]{2,1,0:T(8,128)(2,1)} %param.14) | data formatting | bytes 9216 | tf_op jit(solution)/shard_map/reshape | solution.py:88
  7.8 4.2 %all-to-all-start = ((bf16[4,4,144]{2,1,0:T(4,128)(2,1)}), bf16[4,4,144]{2,1,0:T(4,128)(2,1)S(1)}, u32[]{:S(2)}, u32[]{:S(2)}) async-start(bf16[4,4,144]{2,1,0:T(4,128)(2,1)} %reshape.170), calls=%async_computation | async-start | bytes 16384 | tf_op jit(solution)/shard_map/all_to_all | solution.py:96
  12.1 0.7 all-gather.2.cloned.1.call-update
  12.9 1.3 %reshape.171 = bf16[4,4,144]{2,1,0:T(4,128)(2,1)} reshape(bf16[2,8,144]{2,1,0:T(8,128)(2,1)} %param.13) | data formatting | bytes 9216 | tf_op jit(solution)/shard_map/reshape | solution.py:88
  14.2 1.7 %all-to-all-done = bf16[4,4,144]{2,1,0:T(4,128)(2,1)S(1)} async-done(((bf16[4,4,144]{2,1,0:T(4,128)(2,1)}), bf16[4,4,144]{2,1,0:T(4,128)(2,1)S(1)}, u32[]{:S(2)}, u32[]{:S(2)}) %all-to-all-start) | async-done | bytes 4640 | tf_op jit(solution)/shard_map/all_to_all | solution.py:96
  15.9 3.2 %all-to-all-start.1 = ((bf16[4,4,144]{2,1,0:T(4,128)(2,1)}), bf16[4,4,144]{2,1,0:T(4,128)(2,1)S(1)}, u32[]{:S(2)}, u32[]{:S(2)}) async-start(bf16[4,4,144]{2,1,0:T(4,128)(2,1)} %reshape.171), calls=%async_computation.1 | async-start | bytes 16384 | tf_op jit(solution)/shard_map/all_to_all | solution.py:95
  19.2 3.8 %all-to-all-done.1 = bf16[4,4,144]{2,1,0:T(4,128)(2,1)S(1)} async-done(((bf16[4,4,144]{2,1,0:T(4,128)(2,1)}), bf16[4,4,144]{2,1,0:T(4,128)(2,1)S(1)}, u32[]{:S(2)}, u32[]{:S(2)}) %all-to-all-start.1) | async-done | bytes 4640 | tf_op jit(solution)/shard_map/all_to_all | solution.py:95
  22.9 3.5 %all-to-all-start.2 = ((bf16[4,4,144,128]{3,2,1,0:T(8,128)(2,1)}), bf16[4,4,144,128]{3,2,1,0:T(8,128)(2,1)S(1)}, u32[]{:S(2)}, u32[]{:S(2)}) async-start(bf16[4,4,144,128]{3,2,1,0:T(8,128)(2,1)} %bitcast.130), calls=%async_computation.2 | async-start | bytes 1179648 | tf_op jit(solution)/shard_map/all_to_all | solution.py:93
  26.7 0.9 reduce_window_sum.11
  27.6 0.2 slice_reduce_fusion
  27.7 8.2 %all-to-all-done.2 = bf16[4,4,144,128]{3,2,1,0:T(8,128)(2,1)S(1)} async-done(((bf16[4,4,144,128]{3,2,1,0:T(8,128)(2,1)}), bf16[4,4,144,128]{3,2,1,0:T(8,128)(2,1)S(1)}, u32[]{:S(2)}, u32[]{:S(2)}) %all-to-all-start.2) | async-done | bytes 589856 | tf_op jit(solution)/shard_map/all_to_all | solution.py:93
  35.9 3.5 %all-to-all-start.3 = ((bf16[4,4,144,128]{3,2,1,0:T(8,128)(2,1)}), bf16[4,4,144,128]{3,2,1,0:T(8,128)(2,1)S(1)}, u32[]{:S(2)}, u32[]{:S(2)}) async-start(bf16[4,4,144,128]{3,2,1,0:T(8,128)(2,1)} %bitcast.10), calls=%async_computation.3 | async-start | bytes 1179648 | tf_op jit(solution)/shard_map/all_to_all | solution.py:94
  39.4 0.2 fusion.29
  39.7 0.8 fusion.16
  40.7 8.2 %all-to-all-done.3 = bf16[4,4,144,128]{3,2,1,0:T(8,128)(2,1)S(1)} async-done(((bf16[4,4,144,128]{3,2,1,0:T(8,128)(2,1)}), bf16[4,4,144,128]{3,2,1,0:T(8,128)(2,1)S(1)}, u32[]{:S(2)}, u32[]{:S(2)}) %all-to-all-start.3) | async-done | bytes 589856 | tf_op jit(solution)/shard_map/all_to_all | solution.py:94
  48.9 4.2 %all-to-all-start.4 = ((bf16[4,4,144,128]{3,2,1,0:T(8,128)(2,1)}), bf16[4,4,144,128]{3,2,1,0:T(8,128)(2,1)}, u32[]{:S(2)}, u32[]{:S(2)}) async-start(bf16[4,4,144,128]{3,2,1,0:T(8,128)(2,1)} %bitcast.18), calls=%async_computation.4 | async-start | bytes 1179648 | tf_op jit(solution)/shard_map/all_to_all | solution.py:92
  53.1 0.4 fusion.17
  53.5 2.4 %convolution_bitcast_fusion = f32[9,4,128,128]{3,2,0,1:T(8,128)S(1)} fusion(bf16[4,9,64,128]{3,2,1,0:T(8,128)(2,1)S(1)} %bitcast.123, bf16[4,9,64,128]{3,2,1,0:T(8,128)(2,1)S(1)} %bitcast.120, f32[4,9,64]{2,1,0:T(8,128)S(1)} %exponential_multiply_fusion), kind=kOutput, calls=%fused_computation.19 | convolution fusion | flops 453574656 | bytes 3548160 | tf_op jit(solution)/shard_map/ncsd,ncse->ncde/dot_general | solution.py:33
  55.9 9.3 %while.21 = (s32[]{:T(128)}, f32[4,128,128]{2,1,0:T(8,128)S(1)}, f32[4,128]{1,0:T(4,128)S(1)}, f32[4]{0:T(128)S(1)}, f32[9,4,128,128]{3,2,1,0:T(8,128)}, /*index...) while((s32[]{:T(128)}, f32[4,128,128]{2,1,0:T(8,128)S(1)}, ...), condition=%wide.region_4.5_spmd.clone, body=%wide.region_3.4_spmd.clone.sunk | while | flops 330263 | bytes 1325971 | solution.py:57
  56.0 0.7 bitcast_dynamic-update-slice_fusion.4
  57.0 0.7 bitcast_dynamic-update-slice_fusion.4
  57.7 0.1 fusion.42
  58.0 0.7 bitcast_dynamic-update-slice_fusion.4
  58.7 0.1 fusion.42
  59.0 0.7 bitcast_dynamic-update-slice_fusion.4
  59.8 0.1 fusion.42
  60.1 0.7 bitcast_dynamic-update-slice_fusion.4
  60.8 0.1 fusion.42
  61.1 0.7 bitcast_dynamic-update-slice_fusion.4
  62.2 0.7 bitcast_dynamic-update-slice_fusion.4
  63.2 0.7 bitcast_dynamic-update-slice_fusion.4
  64.2 0.7 bitcast_dynamic-update-slice_fusion.4
  65.3 1.1 %copy.76 = bf16[1,4,4,144,128]{4,3,2,1,0:T(8,128)(2,1)S(1)} copy(bf16[1,4,4,144,128]{4,3,1,2,0:T(8,128)(2,1)} %bitcast.20) | data formatting | bytes 1179648 | tf_op jit(solution)/shard_map/all_to_all | solution.py:92
  66.5 1.0 fusion.27
  67.5 0.7 fusion.31
  68.4 0.9 copy-done.2
  69.2 1.3 %fusion.11 = f32[4,9,64,128]{3,2,1,0:T(8,128)S(1)} fusion(bf16[4,9,64,128]{3,2,1,0:T(8,128)(2,1)S(1)} %bitcast.129, f32[4,9,64]{2,1,0:T(8,128)S(1)} %get-tuple-element.183, f32[9,4,128,128]{3,2,1,0:T(8,128)S(1)} %copy-done.2), kind=kOutput, calls=%fused_computation.21 | convolution fusion | flops 453279744 | bytes 4137984 | tf_op jit(solution)/shard_map/ncpd,ncde->ncpe/dot_general | solution.py:72
  70.6 1.3 %fusion.15 = bf16[4,9,64,128]{3,2,1,0:T(8,128)(2,1)S(1)} fusion(f32[4,9,64,128]{3,2,1,0:T(8,128)S(1)} %fusion.11, f32[4,9,64,64]{2,3,1,0:T(8,128)S(1)} %get-tuple-element.186, bf16[4,9,64,128]{3,2,1,0:T(8,128)(2,1)S(1)} %bitcast.124, f32[4,9,64]{2,1,0:T(8,128)S(1)} %get-tuple-element.182), kind=kOutput, calls=%fused_computation.25 | convolution fusion | flops 227377152 | bytes 2958336 | tf_op jit(solution)/shard_map/ncpq,ncqe->ncpe/dot_general | solution.py:75
  71.9 0.5 copy.79
  72.4 12.6 %all_to_all.72 = bf16[1,4,576,128]{3,1,0,2:T(4,128)(2,1)S(1)} all-to-all(bf16[1,4,576,128]{3,1,0,2:T(4,128)(2,1)S(1)} %copy.79), channel_id=1, replica_groups=mesh['sp'=4,'dp'=8] {'sp'}, dimensions={2} | all-to-all | bytes 1179648 | tf_op jit(solution)/shard_map/all_to_all | solution.py:99
  85.1 0.7 fusion.18
  85.8 0.2 copy.91
  86.0 1.4 %multiply_reduce_fusion = f32[4,4,144]{1,2,0:T(8,128)S(1)} fusion(bf16[1,4,4,144,128]{4,1,3,2,0:T(4,128)(2,1)S(1)} %bitcast.118, f32[4,4,144]{1,2,0:T(8,128)S(1)} %broadcast_multiply_fusion), kind=kLoop, calls=%fused_computation.28 | loop fusion | flops 1177344 | bytes 608256 | tf_op jit(solution)/shard_map/reduce_sum | solution.py:103
  87.5 0.2 copy.92
  87.8 0.8 fusion.22
  88.6 0.2 copy.84
  88.7 3.1 %all-gather.2.cloned.1.call-done = bf16[1024,2048]{1,0:T(8,128)(2,1)} async-done(((bf16[1024,256]{1,0:T(8,128)(2,1)}), bf16[1024,2048]{1,0:T(8,128)(2,1)}) %all-gather.2.cloned.1.call-update) | async-done | bytes 4194320 | tf_op jit(solution)/shard_map/all_gather | solution.py:109
  91.8 4.6 %convolution_convert_fusion = bf16[288,2048]{1,0:T(8,128)(2,1)} fusion(bf16[1024,2048]{1,0:T(8,128)(2,1)} %all-gather.2.cloned.1.call-done, bf16[36,8,8,128]{3,2,1,0:T(8,128)(2,1)S(1)} %bitcast.131), kind=kOutput, calls=%fused_computation.16 | convolution fusion | flops 1208549376 | bytes 5963776 | tf_op jit(solution)/shard_map/dot_general | solution.py:107
  (98 shorter events, 3.2 us)
Async XLA Ops:
  7.8 8.1 %all-to-all-start = ((bf16[4,4,144]{2,1,0:T(4,128)(2,1)}), bf16[4,4,144]{2,1,0:T(4,128)(2,1)S(1)}, u32[]{:S(2)}, u32[]{:S(2)}) async-start(bf16[4,4,144]{2,1,0:T(4,128)(2,1)} %reshape.170), calls=%async_computation | async-start | bytes 16384 | tf_op jit(solution)/shard_map/all_to_all | solution.py:96
  12.1 79.7 %all-gather.2.cloned.1.call-start = ((), (), s32[]{:S(2)}) async-start(), calls=%async_computation.6 | async-start | bytes 4718592 | tf_op jit(solution)/shard_map/all_gather | solution.py:109
  15.9 7.0 %all-to-all-start.1 = ((bf16[4,4,144]{2,1,0:T(4,128)(2,1)}), bf16[4,4,144]{2,1,0:T(4,128)(2,1)S(1)}, u32[]{:S(2)}, u32[]{:S(2)}) async-start(bf16[4,4,144]{2,1,0:T(4,128)(2,1)} %reshape.171), calls=%async_computation.1 | async-start | bytes 16384 | tf_op jit(solution)/shard_map/all_to_all | solution.py:95
  22.9 13.0 %all-to-all-start.2 = ((bf16[4,4,144,128]{3,2,1,0:T(8,128)(2,1)}), bf16[4,4,144,128]{3,2,1,0:T(8,128)(2,1)S(1)}, u32[]{:S(2)}, u32[]{:S(2)}) async-start(bf16[4,4,144,128]{3,2,1,0:T(8,128)(2,1)} %bitcast.130), calls=%async_computation.2 | async-start | bytes 1179648 | tf_op jit(solution)/shard_map/all_to_all | solution.py:93
  35.9 13.0 %all-to-all-start.3 = ((bf16[4,4,144,128]{3,2,1,0:T(8,128)(2,1)}), bf16[4,4,144,128]{3,2,1,0:T(8,128)(2,1)S(1)}, u32[]{:S(2)}, u32[]{:S(2)}) async-start(bf16[4,4,144,128]{3,2,1,0:T(8,128)(2,1)} %bitcast.10), calls=%async_computation.3 | async-start | bytes 1179648 | tf_op jit(solution)/shard_map/all_to_all | solution.py:94
  48.9 16.4 %all-to-all-start.4 = ((bf16[4,4,144,128]{3,2,1,0:T(8,128)(2,1)}), bf16[4,4,144,128]{3,2,1,0:T(8,128)(2,1)}, u32[]{:S(2)}, u32[]{:S(2)}) async-start(bf16[4,4,144,128]{3,2,1,0:T(8,128)(2,1)} %bitcast.18), calls=%async_computation.4 | async-start | bytes 1179648 | tf_op jit(solution)/shard_map/all_to_all | solution.py:92
  53.1 2.8 %copy-start = (bf16[1,4,4,144,128]{4,3,2,1,0:T(8,128)(2,1)}, bf16[1,4,4,144,128]{4,3,2,1,0:T(8,128)(2,1)S(1)}, u32[]{:S(2)}) copy-start(bf16[1,4,4,144,128]{4,3,2,1,0:T(8,128)(2,1)S(1)} %copy.70) | copy-start | bytes 1769476
  67.5 1.7 %copy-start.2 = (f32[9,4,128,128]{3,2,1,0:T(8,128)S(1)}, f32[9,4,128,128]{3,2,1,0:T(8,128)}, u32[]{:S(2)}) copy-start(f32[9,4,128,128]{3,2,1,0:T(8,128)} %get-tuple-element.65) | copy-start | bytes 7077892
  69.2 1.3 %copy-start.1 = (bf16[1,4,4,144,128]{4,3,2,1,0:T(8,128)(2,1)S(1)}, bf16[1,4,4,144,128]{4,3,2,1,0:T(8,128)(2,1)}, u32[]{:S(2)}) copy-start(bf16[1,4,4,144,128]{4,3,2,1,0:T(8,128)(2,1)} %copy-done) | copy-start | bytes 1769476
  85.8 1.9 %copy-start.3 = (bf16[2,8,144,128]{3,2,1,0:T(8,128)(2,1)S(1)}, bf16[2,8,144,128]{3,2,1,0:T(8,128)(2,1)}, u32[]{:S(2)}) copy-start(bf16[2,8,144,128]{3,2,1,0:T(8,128)(2,1)} %param.15) | copy-start | bytes 1769476
  85.8 1.9 %copy-start.4 = (f32[8,128]{1,0:T(8,128)S(1)}, f32[8,128]{1,0:T(8,128)}, u32[]{:S(2)}) copy-start(f32[8,128]{1,0:T(8,128)} %param.16) | copy-start | bytes 12292
Sparse Core Ops, SparseCore 0:
  14.9 76.8 all-gather.1
where the time goes:
time: 104 us; the launch traced here: 103 us
  waiting for transfers between devices  25.6 us (25%)
  starting transfers between devices  18.6 us (18%)
  other arithmetic  14.3 us (14%)
  between operations  13.7 us (13%)
  blocking collectives  12.6 us (12%)
  matrix products  11.4 us (11%)
  local copies, waits for them, and re-layouts  6.74 us (6%)
    all_to_all x1, blocking collectives, body(): lax.all_to_all(cell_out, 'sp', split_axis=2, concat_axis=0, tiled=True)  12.6 us
    all_to_all x1, waiting for transfers between devices, body(): lax.all_to_all(by_rank(keys), 'sp', split_axis=0, concat_axis=2, tiled=True)  8.19 us
    all_to_all x1, waiting for transfers between devices, body(): lax.all_to_all(by_rank(values), 'sp', split_axis=0, concat_axis=2, tiled=...  8.19 us
    dynamic_update_slice x18, other arithmetic, run_cells(): _, (memory_prev, norm_prev, stab_prev) = lax.scan(advance, start, series)  6.71 us
    dot_general x1, matrix products, body(): jnp.dot(hidden, lax.all_gather(out_weight, 'dp', axis=1, tiled=True), pre...  4.59 us
    all_to_all x1, starting transfers between devices, body(): lax.all_to_all(by_rank(forget_gate), 'sp', split_axis=0, concat_axis=2, t...  4.24 us
    all_to_all x1, starting transfers between devices, body(): lax.all_to_all(by_rank(queries), 'sp', split_axis=0, concat_axis=2, tiled...  4.15 us
    all_to_all x1, waiting for transfers between devices, body(): lax.all_to_all(by_rank(in_gate), 'sp', split_axis=0, concat_axis=2, tiled...  3.76 us
  transfers between devices with their start and end apart: 6, of which 5 were waited for; matrix products, arithmetic and copies ran while one was open for 25% of the time, Pallas kernels for 0%

commit v1 on v0

v1 whole, which is shorter than its diff:
```python
import functools

import jax
import jax.numpy as jnp
from jax import lax
from jax.experimental import pallas as pl
from jax.experimental.pallas import tpu as pltpu
from jax.sharding import PartitionSpec as P

norm_eps = 1e-05
MESH = pl.DeviceIdType.MESH
HIGHEST = lax.Precision.HIGHEST
NEG = -1e30


def nt_dot(a, b, precision=None):
    return lax.dot_general(
        a, b, (((1,), (1,)), ((), ())), precision=precision, preferred_element_type=jnp.float32
    )


def tn_dot(a, b):
    return lax.dot_general(a, b, (((0,), (0,)), ((), ())), preferred_element_type=jnp.float32)


def cell_kernel(
    ranks, heads, group,
    q_ref, k_ref, v_ref, ig_ref, fg_ref, og_ref, gain_ref,
    hid_ref,
    c_in, c_out, a_in, a_out, c_loc, n_loc, gate_row, top_row, end_row,
    c_send, c_recv, a_send, a_recv,
):
    rank = lax.axis_index("sp")
    items, span, head_size = q_ref.shape
    groups = items // group
    key_scale = head_size ** (-0.5)
    right = lax.rem(rank + 1, ranks)
    left = lax.rem(rank + ranks - 1, ranks)

    barrier = pltpu.get_barrier_semaphore()
    for neighbour in (left, right):
        pl.semaphore_signal(barrier, inc=1, device_id={"sp": neighbour}, device_id_type=MESH)

    row_i = lax.broadcasted_iota(jnp.int32, (span, span), 0)
    col_i = lax.broadcasted_iota(jnp.int32, (span, span), 1)
    logf = jax.nn.log_sigmoid(fg_ref[...].astype(jnp.float32))
    cumulative = jnp.dot(
        logf, (row_i <= col_i).astype(jnp.float32), precision=HIGHEST,
        preferred_element_type=jnp.float32,
    )
    gate = ig_ref[...].astype(jnp.float32) - cumulative
    top = jnp.max(gate, axis=1, keepdims=True)
    gate_row[...] = gate
    top_row[...] = jnp.broadcast_to(top, (items, head_size))
    end_row[...] = jnp.broadcast_to(cumulative[:, span - 1 :], (items, head_size))
    w_row = jnp.exp(gate - top) * key_scale
    w_col = nt_dot((row_i == col_i).astype(jnp.float32), w_row, precision=HIGHEST)
    for item in range(items):
        weighted = k_ref[item].astype(jnp.float32) * w_col[:, item : item + 1]
        n_loc[pl.ds(item, 1), :] = jnp.sum(weighted, axis=0, keepdims=True)
        c_loc[item] = tn_dot(weighted.astype(jnp.bfloat16), v_ref[item])

    pl.semaphore_wait(barrier, 2)

    def copies(g):
        part = pl.ds(g * group, group)
        return (
            pltpu.make_async_remote_copy(
                src_ref=c_out.at[part], dst_ref=c_in.at[part],
                send_sem=c_send.at[g], recv_sem=c_recv.at[g],
                device_id={"sp": right}, device_id_type=MESH,
            ),
            pltpu.make_async_remote_copy(
                src_ref=a_out.at[part], dst_ref=a_in.at[part],
                send_sem=a_send.at[g], recv_sem=a_recv.at[g],
                device_id={"sp": right}, device_id_type=MESH,
            ),
        )

    def pass_on(g):
        for j in range(group):
            item = g * group + j
            stab = a_in[item, 1:2, :]
            top_here = top_row[pl.ds(item, 1), :]
            new_top = jnp.maximum(stab, top_here)
            keep = jnp.exp(stab - new_top)
            add = jnp.exp(top_here - new_top)
            c_out[item] = (keep * c_in[item].astype(jnp.float32) + add * c_loc[item]).astype(
                jnp.bfloat16
            )
            a_out[item, 0:1, :] = keep * a_in[item, 0:1, :] + add * n_loc[pl.ds(item, 1), :]
            a_out[item, 1:2, :] = end_row[pl.ds(item, 1), :] + new_top
        for copy in copies(g):
            copy.start()

    @pl.when(rank == 0)
    def _():
        c_in[...] = jnp.zeros_like(c_in)
        a_in[...] = jnp.zeros_like(a_in)

        def first(g, carry):
            pass_on(g)
            return carry

        lax.fori_loop(0, groups, first, 0)

    causal = col_i <= row_i

    def step(g, carry):
        local = []
        for j in range(group):
            item = g * group + j
            masked = jnp.where(causal, gate_row[pl.ds(item, 1), :], NEG)
            top_p = jnp.max(masked, axis=1, keepdims=True)
            scores = nt_dot(q_ref[item], k_ref[item]) * (jnp.exp(masked - top_p) * key_scale)
            inner = jnp.dot(
                scores.astype(jnp.bfloat16), v_ref[item], preferred_element_type=jnp.float32
            )
            local.append((top_p, jnp.sum(scores, axis=1, keepdims=True), inner))

        @pl.when(rank > 0)
        def _():
            for copy in copies(g):
                copy.wait_recv()

        @pl.when(jnp.logical_and(rank > 0, rank < ranks - 1))
        def _():
            pass_on(g)

        for j in range(group):
            item = g * group + j
            top_p, den, inner = local[j]
            stab = a_in[item, 1:2, 0:1]
            both = jnp.maximum(top_p, stab)
            w_intra = jnp.exp(top_p - both)
            w_inter = jnp.exp(stab - both)
            query = q_ref[item]
            num = w_inter * jnp.dot(query, c_in[item], preferred_element_type=jnp.float32)
            num = num + w_intra * inner
            carried = jnp.sum(
                query.astype(jnp.float32) * a_in[item, 0:1, :], axis=1, keepdims=True
            )
            den = w_inter * carried + w_intra * den
            cell = num / jnp.maximum(jnp.abs(den), 1.0)
            cell = cell.astype(jnp.bfloat16).astype(jnp.float32)
            centered = cell - jnp.mean(cell, axis=1, keepdims=True)
            variance = jnp.mean(centered * centered, axis=1, keepdims=True)
            head = lax.rem(item, heads)
            seq = item // heads
            normed = centered * lax.rsqrt(variance + norm_eps) * gain_ref[pl.ds(head, 1), :]
            hidden = normed * jax.nn.sigmoid(og_ref[item].astype(jnp.float32))
            hid_ref[
                pl.ds(pl.multiple_of(seq * span, 16), span),
                pl.ds(pl.multiple_of(head * head_size, head_size), head_size),
            ] = hidden.astype(jnp.bfloat16)
        return carry

    lax.fori_loop(0, groups, step, 0)

    @pl.when(rank < ranks - 1)
    def _():
        def finish(g, carry):
            for copy in copies(g):
                copy.wait_send()
            return carry

        lax.fori_loop(0, groups, finish, 0)


def run_cells(ranks, queries, keys, values, in_gate, forget_gate, out_gate, norm_gain):
    seqs, heads, span, head_size = queries.shape
    items = seqs * heads
    group = 4 if heads % 4 == 0 else 1
    groups = items // group
    vmem = pl.BlockSpec(memory_space=pltpu.VMEM)
    flat = lambda a: a.reshape((items,) + a.shape[2:])
    return pl.pallas_call(
        functools.partial(cell_kernel, ranks, heads, group),
        out_shape=jax.ShapeDtypeStruct((seqs * span, heads * head_size), jnp.bfloat16),
        in_specs=[vmem] * 7,
        out_specs=vmem,
        scratch_shapes=[
            pltpu.VMEM((items, head_size, head_size), jnp.bfloat16),
            pltpu.VMEM((items, head_size, head_size), jnp.bfloat16),
            pltpu.VMEM((items, 8, head_size), jnp.float32),
            pltpu.VMEM((items, 8, head_size), jnp.float32),
            pltpu.VMEM((items, head_size, head_size), jnp.float32),
            pltpu.VMEM((items, head_size), jnp.float32),
            pltpu.VMEM((items, span), jnp.float32),
            pltpu.VMEM((items, head_size), jnp.float32),
            pltpu.VMEM((items, head_size), jnp.float32),
            pltpu.SemaphoreType.DMA((groups,)),
            pltpu.SemaphoreType.DMA((groups,)),
            pltpu.SemaphoreType.DMA((groups,)),
            pltpu.SemaphoreType.DMA((groups,)),
        ],
        compiler_params=pltpu.CompilerParams(collective_id=0, has_side_effects=True),
        cost_estimate=pl.CostEstimate(
            flops=items * span * head_size * 2 * 4 * span, bytes_accessed=40000000, transcendentals=0
        ),
    )(
        flat(queries), flat(keys), flat(values), flat(in_gate), flat(forget_gate),
        flat(out_gate), norm_gain,
    )


def solution(mesh):
    ranks = mesh.shape["sp"]

    def body(queries, keys, values, in_gate, forget_gate, out_gate, norm_gain, out_weight):
        seqs, heads, span, head_size = queries.shape
        hidden = run_cells(
            ranks, queries, keys, values, in_gate, forget_gate, out_gate, norm_gain
        )
        result = jnp.dot(
            hidden,
            lax.all_gather(out_weight, "dp", axis=1, tiled=True),
            preferred_element_type=jnp.float32,
        )
        return result.astype(jnp.bfloat16).reshape(seqs, span, -1)

    return jax.shard_map(
        body,
        mesh=mesh,
        in_specs=(
            P("dp", None, "sp", None),
            P("dp", None, "sp", None),
            P("dp", None, "sp", None),
            P("dp", None, "sp"),
            P("dp", None, "sp"),
            P("dp", None, "sp", None),
            P(),
            P(None, "dp"),
        ),
        out_specs=P("dp", "sp", None),
        check_vma=False,
    )
```

time: 104 us -> 98.5 us (0.947)
  waiting for transfers between devices: 25.6 us -> 67.5 us
  starting transfers between devices: 18.6 us -> 0.01 us
  other arithmetic: 14.3 us -> 0 us
  Pallas kernels: 0 us -> 12.8 us
  blocking collectives: 12.6 us -> 0 us
  local copies, waits for them, and re-layouts: 6.74 us -> 0 us
  matrix products: 11.4 us -> 4.78 us
    all_gather x1, waiting for transfers between devices: 3.06 us -> 66.7 us  [body(): lax.all_gather(out_weight, 'dp', axis=1, tiled=True)]
    all_to_all x5 -> x0, waiting for transfers between devices: 21.9 us -> none  [the longest x1 8.19 us: body(): lax.all_to_all(by_rank(keys), 'sp', split_axis=0, concat_axis=2, tiled=True)]
    all_to_all x5 -> x0, starting transfers between devices: 18.6 us -> none  [the longest x1 4.24 us: body(): lax.all_to_all(by_rank(forget_gate), 'sp', split_axis=0, concat_axis=2, t...]
    pallas_call x0 -> x1, Pallas kernels: none -> 12.8 us  [run_cells(): pl.pallas_call(functools.partial(cell_kernel, ranks, heads, group), out_s...]
    all_to_all x1 -> x0, blocking collectives: 12.6 us -> none  [body(): lax.all_to_all(cell_out, 'sp', split_axis=2, concat_axis=0, tiled=True)]
    dot_general x5 -> x0, matrix products: 6.8 us -> none  [the longest x1 2.41 us: run_cells(): jnp.einsum('ncsd,ncse->ncde', weighted, value_f, precision=highest)]
    dynamic_update_slice x18 -> x0, other arithmetic: 6.71 us -> none  [run_cells(): _, (memory_prev, norm_prev, stab_prev) = lax.scan(advance, start, series)]
    reshape x2 -> x0, local copies, waits for them, and re-layouts: 2.61 us -> none  [by_rank(): return array.reshape((rank_count, -1) + array.shape[2:])]
  transfers between devices with their start and end apart: 6 -> 1, of which waited for: 5 -> 1; matrix products, arithmetic and copies ran while one was open for 25% -> 0% of each run, Pallas kernels for 0% -> 13%
where the time goes in v1:
time: 98.5 us; the launch traced here: 98.4 us
  waiting for transfers between devices  67.5 us (69%)
  between operations  13.4 us (14%)
  Pallas kernels  12.8 us (13%)
  matrix products  4.78 us (5%)
    all_gather x1, waiting for transfers between devices, body(): lax.all_gather(out_weight, 'dp', axis=1, tiled=True)  66.7 us
    pallas_call x1, Pallas kernels, run_cells(): pl.pallas_call(functools.partial(cell_kernel, ranks, heads, group), out_s...  12.8 us
    dot_general x1, matrix products, body(): jnp.dot(hidden, lax.all_gather(out_weight, 'dp', axis=1, tiled=True), pre...  4.78 us
  transfers between devices with their start and end apart: 1, of which 1 were waited for; matrix products, arithmetic and copies ran while one was open for 0% of the time, Pallas kernels for 13%

profile of v1, /device:TPU:0, one launch (start us, length us, event | category | flops | bytes accessed | tf_op | source)
XLA Modules:
  0.0 98.4 jit_solution(8333492248611345191)
XLA Ops:
  6.5 0.0 all-gather.2.cloned.1.call-start
  6.5 0.7 all-gather.2.cloned.1.call-update
  7.3 12.8 %shard_map.82 = bf16[288,1024]{1,0:T(8,128)(2,1)} custom-call(bf16[16,144,128]{2,1,0:T(8,128)(2,1)} %bitcast.9, bf16[16,144,128]{2,1,0:T(8,128)(2,1)} %bitcast.10, bf16[16,144,128]{2,1,0:T(8,128)(2,1)} %bitcast.11, bf16[16,144]{1,0:T(8,128)(2,1)} %bitcast.13, bf16[16,144]{1,0:T(8,128)(2,1)} %bitcast.14, bf16[16,144,128]{2,1,0:T(8,128)(2,1)} %bitcast.12, ...), custom_call_target="tpu_custom_call" | custom-call | flops 339738624 | bytes 40000000 | tf_op jit(solution)/shard_map/pallas_call | solution.py:177
  20.0 66.7 %all-gather.2.cloned.1.call-done = bf16[1024,2048]{1,0:T(8,128)(2,1)} async-done(((bf16[1024,256]{1,0:T(8,128)(2,1)}), bf16[1024,2048]{1,0:T(8,128)(2,1)}) %all-gather.2.cloned.1.call-update) | async-done | bytes 4194320 | tf_op jit(solution)/shard_map/all_gather | solution.py:217
  86.8 4.8 %convolution_convert_fusion = bf16[288,2048]{1,0:T(8,128)(2,1)} fusion(bf16[288,1024]{1,0:T(8,128)(2,1)} %shard_map.82, bf16[1024,2048]{1,0:T(8,128)(2,1)} %all-gather.2.cloned.1.call-done), kind=kOutput, calls=%fused_computation | convolution fusion | flops 1208549376 | bytes 5963776 | tf_op jit(solution)/shard_map/dot_general | solution.py:215
Async XLA Ops:
  6.5 80.2 %all-gather.2.cloned.1.call-start = ((), (), s32[]{:S(2)}) async-start(), calls=%async_computation | async-start | bytes 4718592 | tf_op jit(solution)/shard_map/all_gather | solution.py:217
Sparse Core Ops, SparseCore 0:
  9.4 77.3 all-gather.1

commit v2 on v1

v2 whole, which is shorter than its diff:
```python
import functools

import jax
import jax.numpy as jnp
from jax import lax
from jax.experimental import pallas as pl
from jax.experimental.pallas import tpu as pltpu
from jax.sharding import PartitionSpec as P

norm_eps = 1e-05
MESH = pl.DeviceIdType.MESH
HIGHEST = lax.Precision.HIGHEST
NEG = -1e30


def nt_dot(a, b, precision=None):
    return lax.dot_general(
        a, b, (((1,), (1,)), ((), ())), precision=precision, preferred_element_type=jnp.float32
    )


def tn_dot(a, b):
    return lax.dot_general(a, b, (((0,), (0,)), ((), ())), preferred_element_type=jnp.float32)


def split_dot(dot, wide, narrow):
    high = wide.astype(jnp.bfloat16)
    low = (wide - high.astype(jnp.float32)).astype(jnp.bfloat16)
    return dot(high, narrow) + dot(low, narrow)


def nn_dot(a, b):
    return jnp.dot(a, b, preferred_element_type=jnp.float32)


class Cell:
    def __init__(self, ranks, heads, group, refs, hid_ref, state, sems):
        self.ranks, self.heads, self.group = ranks, heads, group
        self.q, self.k, self.v, self.ig, self.fg, self.og, self.gain = refs
        self.hid = hid_ref
        (self.c_in, self.c_out, self.a_in, self.a_out, self.c_loc, self.n_loc, self.gate_row,
         self.top_row, self.end_row) = state
        self.sems = sems
        self.rank = lax.axis_index("sp")
        self.items, self.span, self.size = self.q.shape
        self.groups = self.items // group
        self.scale = self.size ** (-0.5)
        self.right = lax.rem(self.rank + 1, ranks)
        self.row_i = lax.broadcasted_iota(jnp.int32, (self.span, self.span), 0)
        self.col_i = lax.broadcasted_iota(jnp.int32, (self.span, self.span), 1)

    def gates(self):
        items, span, size = self.items, self.span, self.size
        logf = jax.nn.log_sigmoid(self.fg[...].astype(jnp.float32))
        cumulative = jnp.dot(
            logf, (self.row_i <= self.col_i).astype(jnp.float32), precision=HIGHEST,
            preferred_element_type=jnp.float32,
        )
        gate = self.ig[...].astype(jnp.float32) - cumulative
        top = jnp.max(gate, axis=1, keepdims=True)
        self.gate_row[...] = gate
        self.top_row[...] = jnp.broadcast_to(top, (items, size))
        self.end_row[...] = jnp.broadcast_to(cumulative[:, span - 1 :], (items, size))
        w_row = jnp.exp(gate - top) * self.scale
        eye = (self.row_i == self.col_i).astype(jnp.float32)
        self.w_col = nt_dot(eye, w_row, precision=HIGHEST)

    def local_states(self):
        for item in range(self.items):
            weighted = self.k[item].astype(jnp.float32) * self.w_col[:, item : item + 1]
            self.n_loc[pl.ds(item, 1), :] = jnp.sum(weighted, axis=0, keepdims=True)
            self.c_loc[item] = split_dot(tn_dot, weighted, self.v[item])

        @pl.when(self.rank == 0)
        def _():
            self.c_in[...] = jnp.zeros_like(self.c_in)
            self.a_in[...] = jnp.zeros_like(self.a_in)

            def first(g, carry):
                self.pass_on(g)
                return carry

            lax.fori_loop(0, self.groups, first, 0)

    def copies(self, g):
        part = pl.ds(g * self.group, self.group)
        c_send, c_recv, a_send, a_recv = self.sems
        return (
            pltpu.make_async_remote_copy(
                src_ref=self.c_out.at[part], dst_ref=self.c_in.at[part],
                send_sem=c_send.at[g], recv_sem=c_recv.at[g],
                device_id={"sp": self.right}, device_id_type=MESH,
            ),
            pltpu.make_async_remote_copy(
                src_ref=self.a_out.at[part], dst_ref=self.a_in.at[part],
                send_sem=a_send.at[g], recv_sem=a_recv.at[g],
                device_id={"sp": self.right}, device_id_type=MESH,
            ),
        )

    def pass_on(self, g):
        for j in range(self.group):
            item = g * self.group + j
            stab = self.a_in[item, 1:2, :]
            top_here = self.top_row[pl.ds(item, 1), :]
            new_top = jnp.maximum(stab, top_here)
            keep = jnp.exp(stab - new_top)
            add = jnp.exp(top_here - new_top)
            self.c_out[item] = (
                keep * self.c_in[item].astype(jnp.float32) + add * self.c_loc[item]
            ).astype(self.c_out.dtype)
            self.a_out[item, 0:1, :] = (
                keep * self.a_in[item, 0:1, :] + add * self.n_loc[pl.ds(item, 1), :]
            )
            self.a_out[item, 1:2, :] = self.end_row[pl.ds(item, 1), :] + new_top
        for copy in self.copies(g):
            copy.start()

    def step(self, g):
        causal = self.col_i <= self.row_i
        local = []
        for j in range(self.group):
            item = g * self.group + j
            masked = jnp.where(causal, self.gate_row[pl.ds(item, 1), :], NEG)
            top_p = jnp.max(masked, axis=1, keepdims=True)
            scores = nt_dot(self.q[item], self.k[item]) * (jnp.exp(masked - top_p) * self.scale)
            inner = split_dot(nn_dot, scores, self.v[item])
            local.append((top_p, jnp.sum(scores, axis=1, keepdims=True), inner))

        @pl.when(self.rank > 0)
        def _():
            for copy in self.copies(g):
                copy.wait_recv()

        @pl.when(jnp.logical_and(self.rank > 0, self.rank < self.ranks - 1))
        def _():
            self.pass_on(g)

        for j in range(self.group):
            item = g * self.group + j
            top_p, den, inner = local[j]
            stab = self.a_in[item, 1:2, 0:1]
            both = jnp.maximum(top_p, stab)
            w_intra = jnp.exp(top_p - both)
            w_inter = jnp.exp(stab - both)
            query = self.q[item]
            num = w_inter * nn_dot(query, self.c_in[item]) + w_intra * inner
            carried = jnp.sum(
                query.astype(jnp.float32) * self.a_in[item, 0:1, :], axis=1, keepdims=True
            )
            den = w_inter * carried + w_intra * den
            cell = num / jnp.maximum(jnp.abs(den), 1.0)
            cell = cell.astype(jnp.bfloat16).astype(jnp.float32)
            centered = cell - jnp.mean(cell, axis=1, keepdims=True)
            variance = jnp.mean(centered * centered, axis=1, keepdims=True)
            head = lax.rem(item, self.heads)
            seq = item // self.heads
            normed = centered * lax.rsqrt(variance + norm_eps) * self.gain[pl.ds(head, 1), :]
            hidden = normed * jax.nn.sigmoid(self.og[item].astype(jnp.float32))
            self.hid[
                pl.ds(pl.multiple_of(seq * self.span, 16), self.span),
                pl.ds(pl.multiple_of(head * self.size, self.size), self.size),
            ] = hidden.astype(jnp.bfloat16)

    def steps(self, begin, end):
        def one(g, carry):
            self.step(g)
            return carry

        lax.fori_loop(begin, end, one, 0)

    def finish(self):
        @pl.when(self.rank < self.ranks - 1)
        def _():
            def one(g, carry):
                for copy in self.copies(g):
                    copy.wait_send()
                return carry

            lax.fori_loop(0, self.groups, one, 0)


def state_scratch(items, span, size):
    return [
        pltpu.VMEM((items, size, size), jnp.bfloat16),
        pltpu.VMEM((items, size, size), jnp.bfloat16),
        pltpu.VMEM((items, 8, size), jnp.float32),
        pltpu.VMEM((items, 8, size), jnp.float32),
        pltpu.VMEM((items, size, size), jnp.float32),
        pltpu.VMEM((items, size), jnp.float32),
        pltpu.VMEM((items, span), jnp.float32),
        pltpu.VMEM((items, size), jnp.float32),
        pltpu.VMEM((items, size), jnp.float32),
    ]


def cell_kernel(ranks, heads, group, *refs):
    inputs, hid_ref, state, sems = refs[:7], refs[7], refs[8:17], refs[17:21]
    rank = lax.axis_index("sp")
    barrier = pltpu.get_barrier_semaphore()
    for neighbour in (lax.rem(rank + 1, ranks), lax.rem(rank + ranks - 1, ranks)):
        pl.semaphore_signal(barrier, inc=1, device_id={"sp": neighbour}, device_id_type=MESH)
    cell = Cell(ranks, heads, group, inputs, hid_ref, state, sems)
    cell.gates()
    pl.semaphore_wait(barrier, 2)
    cell.local_states()
    cell.steps(0, cell.groups)
    cell.finish()


def nearest(z, nz, k):
    near = jnp.minimum(z, nz - 1 - z)
    half = (k + 1) // 2
    inside = jnp.where(k % 2 == 1, z - half, z + half)
    outside = jnp.where(2 * z < nz, k, nz - 1 - k)
    return jnp.where(k <= 2 * near, inside, outside)


class Gather:
    def __init__(self, nz, ny, w_buf, sems):
        self.nz, self.ny, self.w = nz, ny, w_buf
        (self.z_send, self.z_recv, self.y_send, self.y_recv, self.x_send, self.x_recv,
         self.d_send, self.d_recv) = sems
        self.rank = lax.axis_index("sp")
        self.dp = lax.axis_index("dp")
        self.z, self.y = self.dp // ny, lax.rem(self.dp, ny)
        self.core = lax.rem(self.rank, 2)
        self.plane = lax.rem(self.rank // 2, 2)
        self.sibling = self.rank + 1 - 2 * self.core
        self.across = self.rank + 2 - 4 * self.plane
        self.peer_y = 1 - self.y
        self.rows = w_buf.shape[1] // 2
        self.own = self.dp

    def place(self, k):
        return nearest(self.z, self.nz, k)

    def area(self, piece, part):
        quarter = self.rows // 4
        base = self.core * self.rows
        if part == 1:
            return self.w.at[piece, pl.ds(pl.multiple_of(base + quarter, quarter), 2 * quarter)]
        shift = 3 * self.plane if part == 0 else 3 * (1 - self.plane)
        return self.w.at[piece, pl.ds(pl.multiple_of(base + shift * quarter, quarter), quarter)]

    def copy(self, piece, part, send, recv, where):
        area = self.area(piece, part)
        return pltpu.make_async_remote_copy(
            src_ref=area, dst_ref=area, send_sem=send, recv_sem=recv,
            device_id=where, device_id_type=MESH,
        )

    def z_copy(self, place, part, way):
        ahead = self.z + 1 - 2 * way
        return self.copy(
            place * self.ny + self.y, part, self.z_send.at[place, part, way],
            self.z_recv.at[place, part], {"dp": ahead * self.ny + self.y},
        )

    def y_copy(self, place, mine, part):
        side = self.y if mine else self.peer_y
        return self.copy(
            place * self.ny + side, part, self.y_send.at[place, part],
            self.y_recv.at[place, part], {"dp": self.z * self.ny + self.peer_y},
        )

    def x_copy(self, piece, part):
        return self.copy(
            piece, part, self.x_send.at[piece], self.x_recv.at[piece], {"sp": self.across}
        )

    def d_copy(self, piece, part):
        return self.copy(
            piece, part, self.d_send.at[piece, part], self.d_recv.at[piece, part],
            {"sp": self.sibling},
        )

    def greet(self, barrier, ranks):
        sp = (lax.rem(self.rank + 1, ranks), lax.rem(self.rank + ranks - 1, ranks),
              self.sibling, self.across)
        for one in sp:
            pl.semaphore_signal(barrier, inc=1, device_id={"sp": one}, device_id_type=MESH)
        up, down = lax.rem(self.z + 1, self.nz), lax.rem(self.z + self.nz - 1, self.nz)
        for z, y in ((up, self.y), (down, self.y), (self.z, self.peer_y)):
            pl.semaphore_signal(
                barrier, inc=1, device_id={"dp": z * self.ny + y}, device_id_type=MESH
            )
        return 7

    def start(self):
        for part in (0, 1):
            for way in (0, 1):
                @pl.when(self.z < self.nz - 1 if way == 0 else self.z > 0)
                def _():
                    self.z_copy(self.z, part, way).start()

            self.y_copy(self.z, True, part).start()

    def on_z(self, k):
        place = self.place(k)
        piece = place * self.ny + self.y
        for part in (0, 1):
            self.z_copy(place, part, 0).wait_recv()

            @pl.when(jnp.logical_and(place < self.z, self.z < self.nz - 1))
            def _():
                self.z_copy(place, part, 0).start()

            @pl.when(jnp.logical_and(place > self.z, self.z > 0))
            def _():
                self.z_copy(place, part, 1).start()

            self.y_copy(place, True, part).start()
            if part == 0:
                self.x_copy(piece, 0).start()
            self.d_copy(piece, part).start()

    def on_y(self, k):
        place = self.place(k)
        piece = place * self.ny + self.peer_y
        for part in (0, 1):
            self.y_copy(place, False, part).wait_recv()
            if part == 0:
                self.x_copy(piece, 0).start()
            self.d_copy(piece, part).start()

    def piece_at(self, k, mine):
        return self.place(k) * self.ny + (self.y if mine else self.peer_y)

    def on_x(self, k, mine):
        piece = self.piece_at(k, mine)
        self.x_copy(piece, 2).wait_recv()
        self.d_copy(piece, 2).start()

    def landed(self, k, mine):
        piece = self.piece_at(k, mine)
        other = Gather.__new__(Gather)
        other.__dict__.update(self.__dict__)
        other.core = 1 - self.core
        for part in (0, 1, 2):
            other.d_copy(piece, part).wait_recv()

    def finish(self):
        def z_all(k, carry):
            place = self.place(k)
            for part in (0, 1):
                @pl.when(jnp.logical_and(place <= self.z, self.z < self.nz - 1))
                def _():
                    self.z_copy(place, part, 0).wait_send()

                @pl.when(jnp.logical_and(place >= self.z, self.z > 0))
                def _():
                    self.z_copy(place, part, 1).wait_send()

                self.y_copy(place, True, part).wait_send()
            return carry

        lax.fori_loop(0, self.nz, z_all, 0)

        def others(i, carry):
            piece = lax.rem(self.dp + i, self.nz * self.ny)
            self.x_copy(piece, 0).wait_send()
            for part in (0, 1, 2):
                self.d_copy(piece, part).wait_send()
            return carry

        lax.fori_loop(1, self.nz * self.ny, others, 0)


def whole_kernel(ranks, heads, group, nz, ny, *refs):
    (q_hbm, k_hbm, v_hbm, ig_ref, fg_ref, og_hbm, gain_ref, w_hbm), refs = refs[:8], refs[8:]
    out_hbm, refs = refs[0], refs[1:]
    (q_ref, k_ref, v_ref, og_ref, w_buf, hid_ref, out_ref), refs = refs[:7], refs[7:]
    state, refs = refs[:9], refs[9:]
    chain_sems, refs = refs[:4], refs[4:]
    gather_sems, (load_sems, out_sems) = refs[:8], refs[8:]
    gather = Gather(nz, ny, w_buf, gather_sems)
    barrier = pltpu.get_barrier_semaphore()
    greeted = gather.greet(barrier, ranks)
    w_load = pltpu.make_async_copy(w_hbm, w_buf.at[gather.own], load_sems.at[0])
    loads = [
        pltpu.make_async_copy(src, dst, load_sems.at[1 + i])
        for i, (src, dst) in enumerate(
            ((k_hbm, k_ref), (v_hbm, v_ref), (q_hbm, q_ref), (og_hbm, og_ref))
        )
    ]
    w_load.start()
    for load in loads:
        load.start()
    cell = Cell(
        ranks, heads, group, (q_ref, k_ref, v_ref, ig_ref, fg_ref, og_ref, gain_ref), hid_ref,
        state, chain_sems,
    )
    w_load.wait()
    pl.semaphore_wait(barrier, greeted)
    gather.start()
    cell.gates()
    for load in loads:
        load.wait()
    cell.local_states()
    half = cell.groups // 2

    def out_copy(piece):
        columns = w_buf.shape[2]
        part = pl.ds(pl.multiple_of(piece * columns, columns), columns)
        return pltpu.make_async_copy(
            out_ref.at[:, part], out_hbm.at[:, part], out_sems.at[piece]
        )

    def project(piece):
        columns = w_buf.shape[2]
        part = pl.ds(pl.multiple_of(piece * columns, columns), columns)
        out_ref[:, part] = nn_dot(hid_ref[...], w_buf[piece]).astype(jnp.bfloat16)
        out_copy(piece).start()

    gather.on_z(1)
    gather.on_y(0)
    cell.steps(0, half)
    for k in range(2, nz):
        gather.on_z(k)
        gather.on_y(k - 1)
        gather.on_x(k - 1, True)
        gather.on_x(k - 2, False)
        if k == 2:
            cell.steps(half, cell.groups)
    gather.on_y(nz - 1)
    gather.on_x(nz - 1, True)
    gather.on_x(nz - 2, False)
    project(gather.own)

    def rest(k, carry):
        gather.landed(k, True)
        project(gather.piece_at(k, True))
        gather.landed(k - 1, False)
        project(gather.piece_at(k - 1, False))
        return carry

    lax.fori_loop(1, nz, rest, 0)
    gather.on_x(nz - 1, False)
    gather.landed(nz - 1, False)
    project(gather.piece_at(nz - 1, False))
    cell.finish()
    gather.finish()

    def drain(piece, carry):
        out_copy(piece).wait()
        return carry

    lax.fori_loop(0, nz * ny, drain, 0)


def run_whole(ranks, dps, queries, keys, values, in_gate, forget_gate, out_gate, norm_gain, weight):
    seqs, heads, span, size = queries.shape
    items = seqs * heads
    group = 4
    groups = items // group
    ny = 2
    nz = dps // ny
    rows, columns = weight.shape
    vmem = pl.BlockSpec(memory_space=pltpu.VMEM)
    hbm = pl.BlockSpec(memory_space=pl.ANY)
    flat = lambda a: a.reshape((items,) + a.shape[2:])
    dma = pltpu.SemaphoreType.DMA
    big = pltpu.VMEM((items, span, size), jnp.bfloat16)
    return pl.pallas_call(
        functools.partial(whole_kernel, ranks, heads, group, nz, ny),
        out_shape=jax.ShapeDtypeStruct((seqs * span, dps * columns), jnp.bfloat16),
        in_specs=[hbm, hbm, hbm, vmem, vmem, hbm, vmem, hbm],
        out_specs=hbm,
        scratch_shapes=[
            big, big, big, big,
            pltpu.VMEM((dps, rows, columns), jnp.bfloat16),
            pltpu.VMEM((seqs * span, heads * size), jnp.bfloat16),
            pltpu.VMEM((seqs * span, dps * columns), jnp.bfloat16),
            *state_scratch(items, span, size),
            dma((groups,)), dma((groups,)), dma((groups,)), dma((groups,)),
            dma((nz, 2, 2)), dma((nz, 2)), dma((nz, 2)), dma((nz, 2)),
            dma((dps,)), dma((dps,)), dma((dps, 3)), dma((dps, 3)),
            dma((5,)), dma((dps,)),
        ],
        compiler_params=pltpu.CompilerParams(collective_id=0, has_side_effects=True),
    )(
        flat(queries), flat(keys), flat(values), flat(in_gate), flat(forget_gate),
        flat(out_gate), norm_gain, weight,
    )


def run_cells(ranks, queries, keys, values, in_gate, forget_gate, out_gate, norm_gain):
    seqs, heads, span, head_size = queries.shape
    items = seqs * heads
    group = 4 if heads % 4 == 0 else 1
    groups = items // group
    vmem = pl.BlockSpec(memory_space=pltpu.VMEM)
    flat = lambda a: a.reshape((items,) + a.shape[2:])
    return pl.pallas_call(
        functools.partial(cell_kernel, ranks, heads, group),
        out_shape=jax.ShapeDtypeStruct((seqs * span, heads * head_size), jnp.bfloat16),
        in_specs=[vmem] * 7,
        out_specs=vmem,
        scratch_shapes=[
            *state_scratch(items, span, head_size),
            pltpu.SemaphoreType.DMA((groups,)),
            pltpu.SemaphoreType.DMA((groups,)),
            pltpu.SemaphoreType.DMA((groups,)),
            pltpu.SemaphoreType.DMA((groups,)),
        ],
        compiler_params=pltpu.CompilerParams(collective_id=0, has_side_effects=True),
        cost_estimate=pl.CostEstimate(
            flops=items * span * head_size * 2 * 4 * span, bytes_accessed=40000000, transcendentals=0
        ),
    )(
        flat(queries), flat(keys), flat(values), flat(in_gate), flat(forget_gate),
        flat(out_gate), norm_gain,
    )


def solution(mesh):
    ranks, dps = mesh.shape["sp"], mesh.shape["dp"]

    def body(queries, keys, values, in_gate, forget_gate, out_gate, norm_gain, out_weight):
        seqs, heads, span, head_size = queries.shape
        rows, columns = out_weight.shape
        fits = columns % 128 == 0 and rows % 128 == 0 and dps * rows * columns <= 4 * 2**20
        if ranks == 4 and dps % 2 == 0 and dps >= 6 and heads % 4 == 0 and fits:
            result = run_whole(
                ranks, dps, queries, keys, values, in_gate, forget_gate, out_gate, norm_gain,
                out_weight,
            )
            return result.reshape(seqs, span, -1)
        hidden = run_cells(
            ranks, queries, keys, values, in_gate, forget_gate, out_gate, norm_gain
        )
        result = jnp.dot(
            hidden,
            lax.all_gather(out_weight, "dp", axis=1, tiled=True),
            preferred_element_type=jnp.float32,
        )
        return result.astype(jnp.bfloat16).reshape(seqs, span, -1)

    return jax.shard_map(
        body,
        mesh=mesh,
        in_specs=(
            P("dp", None, "sp", None),
            P("dp", None, "sp", None),
            P("dp", None, "sp", None),
            P("dp", None, "sp"),
            P("dp", None, "sp"),
            P("dp", None, "sp", None),
            P(),
            P(None, "dp"),
        ),
        out_specs=P("dp", "sp", None),
        check_vma=False,
    )
```

time: 98.5 us -> 45.5 us (0.46)
  the two profiles are of different devices: /device:TPU:0 before, /device:TPU:3 now
where the time goes in v2:
time: 45.5 us; the launch traced here: 45.2 us
  Pallas kernels  42.8 us (94%)
  local copies, waits for them, and re-layouts  2.41 us (5%)
    pallas_call x1, Pallas kernels, run_whole(): pl.pallas_call(functools.partial(whole_kernel, ranks, heads, group, nz, n...  42.8 us
    unnamed x1, local copies, waits for them, and re-layouts  2.41 us

profile of v2, /device:TPU:3, one launch (start us, length us, event | category | flops | bytes accessed | tf_op | source)
XLA Modules:
  0.0 45.2 jit_solution(7098872510055693016)
XLA Ops:
  0.0 42.8 %shard_map.82 = bf16[288,2048]{1,0:T(8,128)(2,1)} custom-call(bf16[16,144,128]{2,1,0:T(8,128)(2,1)} %bitcast.8, bf16[16,144,128]{2,1,0:T(8,128)(2,1)} %bitcast.9, bf16[16,144,128]{2,1,0:T(8,128)(2,1)} %bitcast.10, bf16[16,144]{1,0:T(8,128)(2,1)} %bitcast.12, bf16[16,144]{1,0:T(8,128)(2,1)} %bitcast.13, bf16[16,144,128]{2,1,0:T(8,128)(2,1)} %bitcast.11, ...), custom_call_target="tpu_custom_call" | custom-call | tf_op jit(solution)/shard_map/pallas_call | solution.py:465
  42.8 2.4 %copy.10 = bf16[2,144,2048]{2,1,0:T(8,128)(2,1)} copy(bf16[2,144,2048]{2,1,0:T(8,128)(2,1)} %bitcast.7) | data formatting | bytes 2359296

commit v3 on v2

--- a/solution.py
+++ b/solution.py
@@ -39,7 +39,7 @@
         self.q, self.k, self.v, self.ig, self.fg, self.og, self.gain = refs
         self.hid = hid_ref
         (self.c_in, self.c_out, self.a_in, self.a_out, self.c_loc, self.n_loc, self.gate_row,
-         self.top_row, self.end_row) = state
+         self.top_row, self.end_row, self.inner, self.stat) = state
         self.sems = sems
         self.rank = lax.axis_index("sp")
         self.items, self.span, self.size = self.q.shape
@@ -116,35 +116,35 @@
         for copy in self.copies(g):
             copy.start()
 
-    def step(self, g):
+    def intra(self, g):
         causal = self.col_i <= self.row_i
-        local = []
         for j in range(self.group):
             item = g * self.group + j
             masked = jnp.where(causal, self.gate_row[pl.ds(item, 1), :], NEG)
             top_p = jnp.max(masked, axis=1, keepdims=True)
             scores = nt_dot(self.q[item], self.k[item]) * (jnp.exp(masked - top_p) * self.scale)
-            inner = split_dot(nn_dot, scores, self.v[item])
-            local.append((top_p, jnp.sum(scores, axis=1, keepdims=True), inner))
-
-        @pl.when(self.rank > 0)
-        def _():
-            for copy in self.copies(g):
-                copy.wait_recv()
-
-        @pl.when(jnp.logical_and(self.rank > 0, self.rank < self.ranks - 1))
-        def _():
-            self.pass_on(g)
-
+            self.inner[item] = split_dot(nn_dot, scores, self.v[item])
+            self.stat[item, :, 0:1] = top_p
+            self.stat[item, :, 1:2] = jnp.sum(scores, axis=1, keepdims=True)
+
+    def arrive(self, g):
+        for copy in self.copies(g):
+            copy.wait_recv()
+
+    def relay(self, g):
+        self.arrive(g)
+        self.pass_on(g)
+
+    def outcome(self, g):
         for j in range(self.group):
             item = g * self.group + j
-            top_p, den, inner = local[j]
+            top_p, den = self.stat[item, :, 0:1], self.stat[item, :, 1:2]
             stab = self.a_in[item, 1:2, 0:1]
             both = jnp.maximum(top_p, stab)
             w_intra = jnp.exp(top_p - both)
             w_inter = jnp.exp(stab - both)
             query = self.q[item]
-            num = w_inter * nn_dot(query, self.c_in[item]) + w_intra * inner
+            num = w_inter * nn_dot(query, self.c_in[item]) + w_intra * self.inner[item]
             carried = jnp.sum(
                 query.astype(jnp.float32) * self.a_in[item, 0:1, :], axis=1, keepdims=True
             )
@@ -162,12 +162,18 @@
                 pl.ds(pl.multiple_of(head * self.size, self.size), self.size),
             ] = hidden.astype(jnp.bfloat16)
 
-    def steps(self, begin, end):
+    def over(self, work, begin, end):
         def one(g, carry):
-            self.step(g)
+            work(g)
             return carry
 
         lax.fori_loop(begin, end, one, 0)
+
+    def relays(self, ranks, begin, end):
+        for rank in ranks:
+            @pl.when(self.rank == rank)
+            def _():
+                self.over(self.relay if rank < self.ranks - 1 else self.arrive, begin, end)
 
     def finish(self):
         @pl.when(self.rank < self.ranks - 1)
@@ -191,11 +197,13 @@
         pltpu.VMEM((items, span), jnp.float32),
         pltpu.VMEM((items, size), jnp.float32),
         pltpu.VMEM((items, size), jnp.float32),
+        pltpu.VMEM((items, span, size), jnp.float32),
+        pltpu.VMEM((items, span, size), jnp.float32),
     ]
 
 
 def cell_kernel(ranks, heads, group, *refs):
-    inputs, hid_ref, state, sems = refs[:7], refs[7], refs[8:17], refs[17:21]
+    inputs, hid_ref, state, sems = refs[:7], refs[7], refs[8:19], refs[19:23]
     rank = lax.axis_index("sp")
     barrier = pltpu.get_barrier_semaphore()
     for neighbour in (lax.rem(rank + 1, ranks), lax.rem(rank + ranks - 1, ranks)):
@@ -204,7 +212,9 @@
     cell.gates()
     pl.semaphore_wait(barrier, 2)
     cell.local_states()
-    cell.steps(0, cell.groups)
+    cell.over(cell.intra, 0, cell.groups)
+    cell.relays(range(1, ranks), 0, cell.groups)
+    cell.over(cell.outcome, 0, cell.groups)
     cell.finish()
 
 
@@ -238,9 +248,7 @@
     def area(self, piece, part):
         quarter = self.rows // 4
         base = self.core * self.rows
-        if part == 1:
-            return self.w.at[piece, pl.ds(pl.multiple_of(base + quarter, quarter), 2 * quarter)]
-        shift = 3 * self.plane if part == 0 else 3 * (1 - self.plane)
+        shift = (3 * self.plane, 1, 2, 3 * (1 - self.plane))[part]
         return self.w.at[piece, pl.ds(pl.multiple_of(base + shift * quarter, quarter), quarter)]
 
     def copy(self, piece, part, send, recv, where):
@@ -288,7 +296,7 @@
         return 7
 
     def start(self):
-        for part in (0, 1):
+        for part in (0, 1, 2):
             for way in (0, 1):
                 @pl.when(self.z < self.nz - 1 if way == 0 else self.z > 0)
                 def _():
@@ -296,54 +304,52 @@
 
             self.y_copy(self.z, True, part).start()
 
-    def on_z(self, k):
+    def on_z(self, k, part):
         place = self.place(k)
         piece = place * self.ny + self.y
-        for part in (0, 1):
-            self.z_copy(place, part, 0).wait_recv()
-
-            @pl.when(jnp.logical_and(place < self.z, self.z < self.nz - 1))
-            def _():
-                self.z_copy(place, part, 0).start()
-
-            @pl.when(jnp.logical_and(place > self.z, self.z > 0))
-            def _():
-                self.z_copy(place, part, 1).start()
-
-            self.y_copy(place, True, part).start()
-            if part == 0:
-                self.x_copy(piece, 0).start()
-            self.d_copy(piece, part).start()
-
-    def on_y(self, k):
+        self.z_copy(place, part, 0).wait_recv()
+
+        @pl.when(jnp.logical_and(place < self.z, self.z < self.nz - 1))
+        def _():
+            self.z_copy(place, part, 0).start()
+
+        @pl.when(jnp.logical_and(place > self.z, self.z > 0))
+        def _():
+            self.z_copy(place, part, 1).start()
+
+        self.y_copy(place, True, part).start()
+        if part == 0:
+            self.x_copy(piece, 0).start()
+        self.d_copy(piece, part).start()
+
+    def on_y(self, k, part):
         place = self.place(k)
         piece = place * self.ny + self.peer_y
-        for part in (0, 1):
-            self.y_copy(place, False, part).wait_recv()
-            if part == 0:
-                self.x_copy(piece, 0).start()
-            self.d_copy(piece, part).start()
+        self.y_copy(place, False, part).wait_recv()
+        if part == 0:
+            self.x_copy(piece, 0).start()
+        self.d_copy(piece, part).start()
 
     def piece_at(self, k, mine):
         return self.place(k) * self.ny + (self.y if mine else self.peer_y)
 
     def on_x(self, k, mine):
         piece = self.piece_at(k, mine)
-        self.x_copy(piece, 2).wait_recv()
-        self.d_copy(piece, 2).start()
+        self.x_copy(piece, 3).wait_recv()
+        self.d_copy(piece, 3).start()
 
     def landed(self, k, mine):
         piece = self.piece_at(k, mine)
         other = Gather.__new__(Gather)
         other.__dict__.update(self.__dict__)
         other.core = 1 - self.core
-        for part in (0, 1, 2):
+        for part in (0, 1, 2, 3):
             other.d_copy(piece, part).wait_recv()
 
     def finish(self):
         def z_all(k, carry):
             place = self.place(k)
-            for part in (0, 1):
+            for part in (0, 1, 2):
                 @pl.when(jnp.logical_and(place <= self.z, self.z < self.nz - 1))
                 def _():
                     self.z_copy(place, part, 0).wait_send()
@@ -360,7 +366,7 @@
         def others(i, carry):
             piece = lax.rem(self.dp + i, self.nz * self.ny)
             self.x_copy(piece, 0).wait_send()
-            for part in (0, 1, 2):
+            for part in (0, 1, 2, 3):
                 self.d_copy(piece, part).wait_send()
             return carry
 
@@ -369,11 +375,11 @@
 
 def whole_kernel(ranks, heads, group, nz, ny, *refs):
     (q_hbm, k_hbm, v_hbm, ig_ref, fg_ref, og_hbm, gain_ref, w_hbm), refs = refs[:8], refs[8:]
-    out_hbm, refs = refs[0], refs[1:]
-    (q_ref, k_ref, v_ref, og_ref, w_buf, hid_ref, out_ref), refs = refs[:7], refs[7:]
-    state, refs = refs[:9], refs[9:]
+    out_ref, refs = refs[0], refs[1:]
+    (q_ref, k_ref, v_ref, og_ref, w_buf, hid_ref), refs = refs[:6], refs[6:]
+    state, refs = refs[:11], refs[11:]
     chain_sems, refs = refs[:4], refs[4:]
-    gather_sems, (load_sems, out_sems) = refs[:8], refs[8:]
+    gather_sems, load_sems = refs[:8], refs[8]
     gather = Gather(nz, ny, w_buf, gather_sems)
     barrier = pltpu.get_barrier_semaphore()
     greeted = gather.greet(barrier, ranks)
@@ -398,55 +404,74 @@
     for load in loads:
         load.wait()
     cell.local_states()
-    half = cell.groups // 2
-
-    def out_copy(piece):
-        columns = w_buf.shape[2]
-        part = pl.ds(pl.multiple_of(piece * columns, columns), columns)
-        return pltpu.make_async_copy(
-            out_ref.at[:, part], out_hbm.at[:, part], out_sems.at[piece]
-        )
 
     def project(piece):
         columns = w_buf.shape[2]
         part = pl.ds(pl.multiple_of(piece * columns, columns), columns)
         out_ref[:, part] = nn_dot(hid_ref[...], w_buf[piece]).astype(jnp.bfloat16)
-        out_copy(piece).start()
-
-    gather.on_z(1)
-    gather.on_y(0)
-    cell.steps(0, half)
-    for k in range(2, nz):
-        gather.on_z(k)
-        gather.on_y(k - 1)
-        gather.on_x(k - 1, True)
-        gather.on_x(k - 2, False)
-        if k == 2:
-            cell.steps(half, cell.groups)
-    gather.on_y(nz - 1)
+
+    groups = cell.groups
+    mid = groups // 2
+
+    def intra(g):
+        return lambda: cell.intra(g)
+
+    def outcome(g):
+        return lambda: cell.outcome(g)
+
+    def relays(which, begin, end):
+        return lambda: cell.relays(which, begin, end)
+
+    def land(k, mine):
+        def work():
+            gather.landed(k, mine)
+            project(gather.piece_at(k, mine))
+
+        return work
+
+    tasks = []
+    for g in range(groups):
+        tasks.append([intra(g)])
+    tasks[0].append(relays((1,), 0, mid))
+    tasks[1].append(relays((1,), mid, groups))
+    tasks.append([relays((2,), 0, 1)])
+    for g in range(1, groups):
+        tasks.append([relays((2,), g, g + 1), relays((3,), g - 1, g), outcome(g - 1)])
+    tasks.append([relays((3,), groups - 1, groups), outcome(groups - 1)])
+    tasks.append([lambda: project(gather.own)])
+
+    def some(count):
+        for _ in range(min(count, len(tasks))):
+            for task in tasks.pop(0):
+                task()
+
+    for k in range(1, nz):
+        for part in (0, 1, 2):
+            gather.on_z(k, part)
+            gather.on_y(k - 1, part)
+            if k > 1 and part == 1:
+                gather.on_x(k - 1, True)
+                gather.on_x(k - 2, False)
+            some(1)
+    gather.on_y(nz - 1, 0)
+    some(len(tasks))
+    gather.on_y(nz - 1, 1)
     gather.on_x(nz - 1, True)
     gather.on_x(nz - 2, False)
-    project(gather.own)
+    land(1, True)()
+    gather.on_y(nz - 1, 2)
+    land(0, False)()
 
     def rest(k, carry):
-        gather.landed(k, True)
-        project(gather.piece_at(k, True))
-        gather.landed(k - 1, False)
-        project(gather.piece_at(k - 1, False))
+        land(k, True)()
+        land(k - 1, False)()
         return carry
 
-    lax.fori_loop(1, nz, rest, 0)
+    lax.fori_loop(2, nz, rest, 0)
     gather.on_x(nz - 1, False)
-    gather.landed(nz - 1, False)
-    project(gather.piece_at(nz - 1, False))
+    land(nz - 1, False)()
     cell.finish()
     gather.finish()
-
-    def drain(piece, carry):
-        out_copy(piece).wait()
-        return carry
-
-    lax.fori_loop(0, nz * ny, drain, 0)
 
 
 def run_whole(ranks, dps, queries, keys, values, in_gate, forget_gate, out_gate, norm_gain, weight):
@@ -464,19 +489,18 @@
     big = pltpu.VMEM((items, span, size), jnp.bfloat16)
     return pl.pallas_call(
         functools.partial(whole_kernel, ranks, heads, group, nz, ny),
-        out_shape=jax.ShapeDtypeStruct((seqs * span, dps * columns), jnp.bfloat16),
+        out_shape=pltpu.VMEM((seqs * span, dps * columns), jnp.bfloat16),
         in_specs=[hbm, hbm, hbm, vmem, vmem, hbm, vmem, hbm],
-        out_specs=hbm,
+        out_specs=vmem,
         scratch_shapes=[
             big, big, big, big,
             pltpu.VMEM((dps, rows, columns), jnp.bfloat16),
             pltpu.VMEM((seqs * span, heads * size), jnp.bfloat16),
-            pltpu.VMEM((seqs * span, dps * columns), jnp.bfloat16),
             *state_scratch(items, span, size),
             dma((groups,)), dma((groups,)), dma((groups,)), dma((groups,)),
-            dma((nz, 2, 2)), dma((nz, 2)), dma((nz, 2)), dma((nz, 2)),
-            dma((dps,)), dma((dps,)), dma((dps, 3)), dma((dps, 3)),
-            dma((5,)), dma((dps,)),
+            dma((nz, 3, 2)), dma((nz, 3)), dma((nz, 3)), dma((nz, 3)),
+            dma((dps,)), dma((dps,)), dma((dps, 4)), dma((dps, 4)),
+            dma((5,)),
         ],
         compiler_params=pltpu.CompilerParams(collective_id=0, has_side_effects=True),
     )(

time: 45.5 us -> 34.7 us (0.76)
  the two profiles are of different devices: /device:TPU:3 before, /device:TPU:0 now
where the time goes in v3:
time: 34.7 us; the launch traced here: 34.4 us
  Pallas kernels  33.4 us (96%)
  local copies, waits for them, and re-layouts  1.02 us (3%)
    pallas_call x1, Pallas kernels, run_whole(): pl.pallas_call(functools.partial(whole_kernel, ranks, heads, group, nz, n...  33.4 us
    unnamed x1, local copies, waits for them, and re-layouts  1.02 us

profile of v3, /device:TPU:0, one launch (start us, length us, event | category | flops | bytes accessed | tf_op | source)
XLA Modules:
  0.0 34.4 jit_solution(14419282153734955332)
XLA Ops:
  0.0 33.4 %shard_map.82 = bf16[288,2048]{1,0:T(8,128)(2,1)S(1)} custom-call(bf16[16,144,128]{2,1,0:T(8,128)(2,1)} %bitcast.8, bf16[16,144,128]{2,1,0:T(8,128)(2,1)} %bitcast.9, bf16[16,144,128]{2,1,0:T(8,128)(2,1)} %bitcast.10, bf16[16,144]{1,0:T(8,128)(2,1)} %bitcast.12, bf16[16,144]{1,0:T(8,128)(2,1)} %bitcast.13, bf16[16,144,128]{2,1,0:T(8,128)(2,1)} %bitcast.11, ...), custom_call_target="tpu_custom_call" | custom-call | tf_op jit(solution)/shard_map/pallas_call | solution.py:490
  33.4 1.0 %copy.10 = bf16[2,144,2048]{2,1,0:T(8,128)(2,1)} copy(bf16[2,144,2048]{2,1,0:T(8,128)(2,1)S(1)} %bitcast.7) | data formatting | bytes 2359296

commit v4 on v3

--- a/solution.py
+++ b/solution.py
@@ -245,11 +245,15 @@
     def place(self, k):
         return nearest(self.z, self.nz, k)
 
+    def span_of(self, part):
+        quarter = self.rows // 4
+        if part == 4:
+            return pl.ds(pl.multiple_of((1 - self.core) * self.rows, self.rows), self.rows)
+        shift = (3 * self.plane, 1, 2, 3 * (1 - self.plane))[part]
+        return pl.ds(pl.multiple_of(self.core * self.rows + shift * quarter, quarter), quarter)
+
     def area(self, piece, part):
-        quarter = self.rows // 4
-        base = self.core * self.rows
-        shift = (3 * self.plane, 1, 2, 3 * (1 - self.plane))[part]
-        return self.w.at[piece, pl.ds(pl.multiple_of(base + shift * quarter, quarter), quarter)]
+        return self.w.at[piece, self.span_of(part)]
 
     def copy(self, piece, part, send, recv, where):
         area = self.area(piece, part)
@@ -295,14 +299,13 @@
             )
         return 7
 
-    def start(self):
-        for part in (0, 1, 2):
-            for way in (0, 1):
-                @pl.when(self.z < self.nz - 1 if way == 0 else self.z > 0)
-                def _():
-                    self.z_copy(self.z, part, way).start()
-
-            self.y_copy(self.z, True, part).start()
+    def start(self, part):
+        for way in (0, 1):
+            @pl.when(self.z < self.nz - 1 if way == 0 else self.z > 0)
+            def _():
+                self.z_copy(self.z, part, way).start()
+
+        self.y_copy(self.z, True, part).start()
 
     def on_z(self, k, part):
         place = self.place(k)
@@ -374,34 +377,45 @@
 
 
 def whole_kernel(ranks, heads, group, nz, ny, *refs):
-    (q_hbm, k_hbm, v_hbm, ig_ref, fg_ref, og_hbm, gain_ref, w_hbm), refs = refs[:8], refs[8:]
+    (q_hbm, k_hbm, v_hbm, ig_hbm, fg_hbm, og_hbm, gain_hbm, w_hbm), refs = refs[:8], refs[8:]
     out_ref, refs = refs[0], refs[1:]
-    (q_ref, k_ref, v_ref, og_ref, w_buf, hid_ref), refs = refs[:6], refs[6:]
+    (q_ref, k_ref, v_ref, og_ref, ig_ref, fg_ref, gain_ref, w_buf, hid_ref), refs = (
+        refs[:9], refs[9:]
+    )
     state, refs = refs[:11], refs[11:]
     chain_sems, refs = refs[:4], refs[4:]
     gather_sems, load_sems = refs[:8], refs[8]
     gather = Gather(nz, ny, w_buf, gather_sems)
     barrier = pltpu.get_barrier_semaphore()
     greeted = gather.greet(barrier, ranks)
-    w_load = pltpu.make_async_copy(w_hbm, w_buf.at[gather.own], load_sems.at[0])
+    w_loads = [
+        pltpu.make_async_copy(
+            w_hbm.at[gather.span_of(part)], w_buf.at[gather.own, gather.span_of(part)],
+            load_sems.at[part],
+        )
+        for part in range(5)
+    ]
     loads = [
-        pltpu.make_async_copy(src, dst, load_sems.at[1 + i])
+        pltpu.make_async_copy(src, dst, load_sems.at[5 + i])
         for i, (src, dst) in enumerate(
-            ((k_hbm, k_ref), (v_hbm, v_ref), (q_hbm, q_ref), (og_hbm, og_ref))
+            ((fg_hbm, fg_ref), (ig_hbm, ig_ref), (k_hbm, k_ref), (v_hbm, v_ref), (q_hbm, q_ref),
+             (gain_hbm, gain_ref), (og_hbm, og_ref))
         )
     ]
-    w_load.start()
-    for load in loads:
+    for load in w_loads[:3] + loads + w_loads[3:]:
         load.start()
     cell = Cell(
         ranks, heads, group, (q_ref, k_ref, v_ref, ig_ref, fg_ref, og_ref, gain_ref), hid_ref,
         state, chain_sems,
     )
-    w_load.wait()
     pl.semaphore_wait(barrier, greeted)
-    gather.start()
+    for part in (0, 1, 2):
+        w_loads[part].wait()
+        gather.start(part)
+    for load in loads[:2]:
+        load.wait()
     cell.gates()
-    for load in loads:
+    for load in loads[2:] + w_loads[3:]:
         load.wait()
     cell.local_states()
 
@@ -455,11 +469,10 @@
             some(1)
     gather.on_y(nz - 1, 0)
     some(len(tasks))
+    land(1, True)()
     gather.on_y(nz - 1, 1)
     gather.on_x(nz - 1, True)
     gather.on_x(nz - 2, False)
-    land(1, True)()
-    gather.on_y(nz - 1, 2)
     land(0, False)()
 
     def rest(k, carry):
@@ -467,8 +480,10 @@
         land(k - 1, False)()
         return carry
 
-    lax.fori_loop(2, nz, rest, 0)
+    lax.fori_loop(2, nz - 1, rest, 0)
+    gather.on_y(nz - 1, 2)
     gather.on_x(nz - 1, False)
+    rest(nz - 1, 0)
     land(nz - 1, False)()
     cell.finish()
     gather.finish()
@@ -490,17 +505,20 @@
     return pl.pallas_call(
         functools.partial(whole_kernel, ranks, heads, group, nz, ny),
         out_shape=pltpu.VMEM((seqs * span, dps * columns), jnp.bfloat16),
-        in_specs=[hbm, hbm, hbm, vmem, vmem, hbm, vmem, hbm],
+        in_specs=[hbm] * 8,
         out_specs=vmem,
         scratch_shapes=[
             big, big, big, big,
+            pltpu.VMEM((items, span), jnp.bfloat16),
+            pltpu.VMEM((items, span), jnp.bfloat16),
+            pltpu.VMEM((heads, size), jnp.float32),
             pltpu.VMEM((dps, rows, columns), jnp.bfloat16),
             pltpu.VMEM((seqs * span, heads * size), jnp.bfloat16),
             *state_scratch(items, span, size),
             dma((groups,)), dma((groups,)), dma((groups,)), dma((groups,)),
             dma((nz, 3, 2)), dma((nz, 3)), dma((nz, 3)), dma((nz, 3)),
             dma((dps,)), dma((dps,)), dma((dps, 4)), dma((dps, 4)),
-            dma((5,)),
+            dma((12,)),
         ],
         compiler_params=pltpu.CompilerParams(collective_id=0, has_side_effects=True),
     )(

time: 34.7 us -> 34 us (0.980)
  Pallas kernels: 33.4 us -> 32.9 us
    pallas_call x1, Pallas kernels: 33.4 us -> 32.9 us  [run_whole(): pl.pallas_call(functools.partial(whole_kernel, ranks, heads, group, nz, n...]
where the time goes in v4:
time: 34 us; the launch traced here: 33.9 us
  Pallas kernels  32.9 us (97%)
  local copies, waits for them, and re-layouts  1.02 us (3%)
    pallas_call x1, Pallas kernels, run_whole(): pl.pallas_call(functools.partial(whole_kernel, ranks, heads, group, nz, n...  32.9 us
    unnamed x1, local copies, waits for them, and re-layouts  1.02 us

profile of v4, /device:TPU:0, one launch (start us, length us, event | category | flops | bytes accessed | tf_op | source)
XLA Modules:
  0.0 33.9 jit_solution(17494688524471359317)
XLA Ops:
  0.0 32.9 %shard_map.82 = bf16[288,2048]{1,0:T(8,128)(2,1)S(1)} custom-call(bf16[16,144,128]{2,1,0:T(8,128)(2,1)} %bitcast.8, bf16[16,144,128]{2,1,0:T(8,128)(2,1)} %bitcast.9, bf16[16,144,128]{2,1,0:T(8,128)(2,1)} %bitcast.10, bf16[16,144]{1,0:T(8,128)(2,1)} %bitcast.12, bf16[16,144]{1,0:T(8,128)(2,1)} %bitcast.13, bf16[16,144,128]{2,1,0:T(8,128)(2,1)} %bitcast.11, ...), custom_call_target="tpu_custom_call" | custom-call | tf_op jit(solution)/shard_map/pallas_call | solution.py:505
  32.9 1.0 %copy.10 = bf16[2,144,2048]{2,1,0:T(8,128)(2,1)} copy(bf16[2,144,2048]{2,1,0:T(8,128)(2,1)S(1)} %bitcast.7) | data formatting | bytes 2359296
